TPU v7x, 32 devices: a whole 2x2x4 slice. The times are simulated.
32 devices in a mesh: rep: 2 (over x), fs: 8 (over z, y), tp: 2 (over core).
Axes of the slice: x: 2, y: 2, z: 4, core: 2. Of those that a mesh axis runs over, the one named last changes fastest.
Arguments:
- tokens: bfloat16 [8192, 2048], P(('rep', 'fs'), 'tp'), may hold values from -6 to 6
- mix_gain: float32 [2048], replicated, may hold values from 0.1 to 1.9
- lru_input: float32 [2048, 2048], P('fs', 'tp'), may hold values from -0.125 to 0.125
- lru_gate: float32 [2048, 2048], P('fs', 'tp'), may hold values from -0.125 to 0.125
- lru_input_scale: float32 [2048], P('tp'), may hold values from 0.5 to 2
- lru_gate_scale: float32 [2048], P('tp'), may hold values from 0.5 to 2
- conv_weight: float32 [4, 2048], P(None, 'tp'), may hold values from -3 to 3
- recur_gate: float32 [32, 64, 64], P('tp'), may hold values from -0.75 to 0.75
- input_gate: float32 [32, 64, 64], P('tp'), may hold values from -0.75 to 0.75
- decay_rate: float32 [2048], P('tp'), may hold values from 3.5 to 9
- extra_decay: float32 [8192], P(('rep', 'fs')), may hold values from 0.0003 to 2.1
- lru_output: float32 [2048, 2048], P('tp', 'fs'), may hold values from -0.125 to 0.125
- lru_output_scale: float32 [2048], replicated, may hold values from 0.5 to 2
- ffn_gain: float32 [2048], replicated, may hold values from 0.1 to 1.9
- ffn_gate: float32 [2048, 2816], P('fs', 'tp'), may hold values from -0.125 to 0.125
- ffn_up: float32 [2048, 2816], P('fs', 'tp'), may hold values from -0.125 to 0.125
- ffn_gate_scale: float32 [2816], P('tp'), may hold values from 0.5 to 2
- ffn_up_scale: float32 [2816], P('tp'), may hold values from 0.5 to 2
- ffn_down: float32 [2816, 2048], P('tp', 'fs'), may hold values from -0.109375 to 0.109375
- ffn_down_scale: float32 [2048], replicated, may hold values from 0.5 to 2
Outputs:
- layer_out: bfloat16 [8192, 2048], P(('rep', 'fs'), 'tp')
All inputs are finite; a program needn't handle non-finite values.
Results may differ from a plain program's by a relative error of at most 0.02.
Values may be sent and summed in bfloat16 or wider, within the bound.
A program may use at most 192 MiB of HBM per device.

v0:
```python
import functools

import jax
import jax.numpy as jnp
from jax import lax
from jax.experimental import pallas as pl
from jax.experimental.pallas import tpu as pltpu
from jax.sharding import PartitionSpec as P

EPS = 1e-06
RATE = 8.0
LANES = 128
FIRST = 6.0
RATE_BOTH = 23300.0
HOP = 22.5
DOT = (1.5, 0.0, 2.2)
MESH = pl.DeviceIdType.MESH


def scoped(name):
    def wrap(f):
        def inner(*args):
            with jax.named_scope(name + "".join(f"_{a}" for a in args if isinstance(a, int))):
                return f(*args)

        return inner

    return wrap


def sigmoid(v):
    return 1.0 / (1.0 + jnp.exp(-v))


def rec_block(values, gate, taps, maps, rate, extra):
    length = values.shape[0]
    ntaps = taps.shape[0]
    row = lax.broadcasted_iota(jnp.int32, values.shape, 0)
    conv = taps[ntaps - 1 : ntaps, :] * values
    for back in range(1, ntaps):
        moved = jnp.where(row >= back, pltpu.roll(values, back, 0), 0.0)
        conv = conv + taps[ntaps - 1 - back : ntaps - back, :] * moved
    mapped = jnp.dot(
        conv, maps, preferred_element_type=jnp.float32, precision=lax.Precision.HIGHEST
    )
    recur = sigmoid(mapped[:, :LANES])
    ingate = sigmoid(mapped[:, LANES:])
    log_rate = rate * recur - extra
    a = jnp.exp(log_rate)
    u = -2.0 * log_rate
    series = u * (1 - u / 2 * (1 - u / 3 * (1 - u / 4 * (1 - u / 5 * (1 - u / 6)))))
    b = jnp.sqrt(jnp.where(u < 0.25, series, 1.0 - jnp.exp(-u))) * (ingate * conv)
    inner = row % 8
    for s in (1, 2, 4):
        keep = inner >= s
        b = jnp.where(keep, a * pltpu.roll(b, s, 0) + b, b)
        a = jnp.where(keep, a * pltpu.roll(a, s, 0), a)
    groups = length // 8
    last_a = a.reshape(groups, 8, LANES)
    last_b = b.reshape(groups, 8, LANES)
    ca = jnp.broadcast_to(last_a[:, 7:8, :], last_a.shape).reshape(length, LANES)
    cb = jnp.broadcast_to(last_b[:, 7:8, :], last_b.shape).reshape(length, LANES)
    s = 8
    while s < length:
        cb_new = ca[s:] * cb[:-s] + cb[s:]
        ca_new = ca[s:] * ca[:-s]
        cb = jnp.concatenate([cb[:s], cb_new], axis=0)
        ca = jnp.concatenate([ca[:s], ca_new], axis=0)
        s *= 2
    state = jnp.concatenate([b[:8], a[8:] * cb[:-8] + b[8:]], axis=0)
    gelu = 0.5 * gate * (1.0 + jnp.tanh(0.7978845608028654 * (gate + 0.044715 * gate * gate * gate)))
    return (state * gelu).astype(jnp.bfloat16)


def layer_kernel(
    ny,
    nz,
    tokens,
    lru_input,
    lru_gate,
    lru_output,
    ffn_gate,
    ffn_up,
    ffn_down,
    extra_ref,
    mgain_ref,
    fgain_ref,
    iscale_ref,
    gscale_ref,
    oscale_ref,
    fscale_ref,
    dscale_ref,
    taps_ref,
    rmap_ref,
    imap_ref,
    decay_ref,
    o_ref,
    tok,
    ex,
    nrm,
    b0,
    b1,
    b2,
    b3,
    st_mix,
    st_out,
    st_down,
    acc,
    gated,
    hid,
    part,
    thr_s,
    thr_r,
    xs,
    xr,
    maps,
    rates,
    guscale,
    lsem,
    us,
    ur,
    ds,
    dr,
    ys,
    yr,
    ts,
    tr,
    ps,
    pr,
    xss,
    xrs,
    ms,
    mr,
):
    f32, bf16 = jnp.float32, jnp.bfloat16
    fs = ny * nz
    length, columns = tokens.shape
    c = lru_input.shape[0]
    hb = columns // c
    width = gated.shape[2]
    hidden = hid.shape[2]
    rep, tp, me = lax.axis_index("rep"), lax.axis_index("tp"), lax.axis_index("fs")
    z, y = me // ny, me % ny
    buf = (b0, b1, b2, b3)
    over_x = {"rep": 1 - rep}
    over_tp = {"tp": 1 - tp}
    over_y = {"fs": z * ny + (1 - y)}
    half = nz // 2
    plan = (
        ((96, False), (112, False), (48, True)),
        ((416, False), (96, True)),
        ((96, False), (96, False), (64, True)),
        ((704, False),),
    )
    groups = []
    for b, parts in enumerate(plan):
        row, rows = 0, buf[b].shape[1]
        whole_rows = sum(n for n, _ in parts)
        for i, (n, both) in enumerate(parts):
            n = rows - row if i + 1 == len(parts) else max(16, n * rows // whole_rows // 16 * 16)
            groups.append((b, row, n, both and ny > 1))
            row += n

    clock = [0.0]
    eta, slots, at_time = {}, [], FIRST
    for g, (b, _, n, both) in enumerate(groups):
        size = n * buf[b].shape[2] * (2 if both else 1)
        for k in range(1, nz):
            at_time += size / RATE_BOTH
            eta[g, k] = at_time
            slots.append((g, k))

    def copy(src, dst, s, r, where):
        return pltpu.make_async_remote_copy(
            src_ref=src, dst_ref=dst, send_sem=s, recv_sem=r, device_id=where, device_id_type=MESH
        )

    def piece(g, at, w):
        b, row, rows, _ = groups[g]
        return buf[b].at[at * ny + (y if w == 0 else 1 - y), pl.ds(row, rows)]

    def tracks(g):
        return (0, 1) if groups[g][3] else (0,)

    def up(g, w, k, at):
        p = piece(g, at, w)
        return copy(p, p, us.at[g, w, k], ur.at[g, w, k], {"fs": lax.rem(z + 1, nz) * ny + y})

    def down_z(g, w, k, at):
        p = piece(g, at, w)
        return copy(
            p, p, ds.at[g, w, k], dr.at[g, w, k], {"fs": lax.rem(z + nz - 1, nz) * ny + y}
        )

    def from_z(d):
        return lax.rem(z - d + nz, nz)

    def over(g, d, w=0):
        p = piece(g, from_z(d), w)
        return copy(p, p, ys.at[g, d], yr.at[g, d], over_y)

    def can_up(k):
        return (z + 1 < nz) & (z >= k - 1)

    def can_down(k):
        return (z > 0) & (z + k <= nz)

    def own_y(g):
        if g < len(groups) and ny > 1:
            over(g, 0).start()

    def own_z(g):
        if g < len(groups):
            if groups[g][3]:
                over(g, 0, 1).wait_recv()
            for w in tracks(g):

                @pl.when(can_up(1))
                def _():
                    up(g, w, 1, z).start()

                @pl.when(can_down(1))
                def _():
                    down_z(g, w, 1, z).start()

    @scoped("slot")
    def slot(g, k):
        if k == nz - 1:
            own_z(g + 1)
            own_y(g + 2)

        @pl.when(z >= k)
        def _():
            for w in tracks(g):
                up(g, w, k, z - k).wait_recv()
                if k + 1 < nz:

                    @pl.when(can_up(k + 1))
                    def _():
                        up(g, w, k + 1, z - k).start()

            if ny > 1 and not groups[g][3]:
                over(g, k).start()

        @pl.when(z + k < nz)
        def _():
            for w in tracks(g):
                down_z(g, w, k, z + k).wait_recv()
                if k + 1 < nz:

                    @pl.when(can_down(k + 1))
                    def _():
                        down_z(g, w, k + 1, z + k).start()

            if ny > 1 and not groups[g][3]:
                over(g, nz - k).start()

    def next_slot():
        key = slots.pop(0)
        clock[0] = max(clock[0], eta[key])
        slot(*key)

    def pump(until):
        while slots and eta[slots[0]] <= until:
            next_slot()

    def need(b, k):
        g = max(i for i, group in enumerate(groups) if group[0] == b)
        while slots and slots[0] <= (g, k):
            next_slot()

    def run(cost, f, *args):
        pump(clock[0] + cost / 2)
        f(*args)
        clock[0] += cost

    def wait_until(when, f, *args):
        pump(when)
        f(*args)
        clock[0] = max(clock[0], when)

    def nth(i):
        near = jnp.minimum(z, nz - 1 - z)
        step = i // 2 + 1
        both = z - step if i % 2 == 0 else z + step
        far = i - near + 1
        rest = jnp.where(z > nz - 1 - z, z - far, z + far)
        return jnp.where(i < 2 * near, both, rest)

    def stage(src, dst, i):
        return pltpu.make_async_copy(src, dst, lsem.at[i])

    mine_cols = pl.ds(pl.multiple_of(rep * width, LANES), width)
    loads = [
        stage(lru_input.at[:, mine_cols], st_mix.at[0], 0),
        stage(lru_gate.at[:, mine_cols], st_mix.at[1], 1),
        stage(tokens, tok.at[0, tp], 2),
        stage(lru_output.at[pl.ds(pl.multiple_of(rep * width, 8), width)], st_out, 3),
        stage(ffn_gate, acc.at[0, :c], 4),
        stage(ffn_up, acc.at[1, :c], 5),
        stage(ffn_down.at[pl.ds(pl.multiple_of(rep * hidden, 8), hidden)], st_down, 6),
    ]
    for load in loads:
        load.start()

    barrier = pltpu.get_barrier_semaphore()

    def greet(where):
        pl.semaphore_signal(barrier, inc=1, device_id=where, device_id_type=MESH)

    greet(over_x)
    greet(over_tp)
    if ny > 1:
        greet(over_y)
    pl.when(z + 1 < nz)(lambda: greet({"fs": lax.rem(z + 1, nz) * ny + y}))
    pl.when(z > 0)(lambda: greet({"fs": lax.rem(z + nz - 1, nz) * ny + y}))

    loads[0].wait()
    loads[1].wait()
    b0[me, :, :width] = st_mix[0].astype(bf16)
    b0[me, :, width:] = st_mix[1].astype(bf16)
    ex[0] = jnp.broadcast_to(extra_ref[...], ex.shape[1:])
    loads[2].wait()

    along_z = jnp.where(z > 0, 1, 0) + jnp.where(z + 1 < nz, 1, 0)
    pl.semaphore_wait(barrier, (3 if ny > 1 else 2) + along_z)

    def tok_copy(s, i, where, to):
        return copy(tok.at[s, tp], tok.at[to, tp], ts.at[i], tr.at[i], where)

    tok_tp = tok_copy(0, 0, over_tp, 0)
    tok_x = tok_copy(0, 1, over_x, 1)
    tok_xtp = tok_copy(1, 2, over_tp, 1)
    extra_x = copy(ex.at[0], ex.at[1], ts.at[3], tr.at[3], over_x)
    own_z(0)
    own_y(0)
    tok_tp.start()
    tok_x.start()
    extra_x.start()
    loads[3].wait()
    b1[me] = st_out[...].astype(bf16)
    own_y(1)

    @scoped("wait")
    def arrived(c):
        c.wait_recv()

    main = hidden // LANES * LANES
    rest = hidden - main

    @scoped("pack")
    def pack():
        loads[4].wait()
        loads[5].wait()
        step = 32

        def mine(v):
            return jnp.where(rep == 0, v, pltpu.roll(v, hidden, 1))

        def pair(g, u):
            g, u = mine(g), mine(u)
            out = [g[:, :main], u[:, :main]]
            if rest:
                g, u = g[:, main : main + LANES], u[:, main : main + LANES]
                lane = lax.broadcasted_iota(jnp.int32, g.shape, 1)
                out.append(jnp.where(lane < rest, g, pltpu.roll(u, rest, 1)))
            return out

        def body(i, _):
            r = pl.ds(pl.multiple_of(i * step, step), step)
            out = pair(acc[0, r, :], acc[1, r, :])
            b2[me, r, :main] = out[0].astype(bf16)
            b2[me, r, main : 2 * main] = out[1].astype(bf16)
            if rest:
                b2[me, r, 2 * main :] = out[2].astype(bf16)
            return 0

        lax.fori_loop(0, c // step, body, 0)
        wide = (8, 2 * hidden)
        out = pair(
            jnp.broadcast_to(fscale_ref[0:1, :], wide), jnp.broadcast_to(fscale_ref[1:2, :], wide)
        )
        guscale[:, :main] = out[0]
        guscale[:, main : 2 * main] = out[1]
        if rest:
            guscale[:, 2 * main :] = out[2]
        loads[6].wait()
        b3[me] = st_down[...].astype(bf16)

    @scoped("tables")
    def tables():
        v = -decay_ref[:, mine_cols]
        e = jnp.exp(-jnp.abs(v))
        q = e / (2.0 + e)
        p = q * q
        poly = jnp.full_like(p, 1.0 / 17)
        for odd in range(15, 0, -2):
            poly = poly * p + 1.0 / odd
        rates[...] = -RATE * (jnp.maximum(v, 0.0) + 2.0 * q * poly)
        bdim = rmap_ref.shape[1]
        per = LANES // bdim
        zero = jnp.zeros((bdim, bdim), f32)
        for i in range(width // LANES):
            for p_ in range(per):
                for k, ref in enumerate((rmap_ref, imap_ref)):
                    block = ref[rep * (width // bdim) + i * per + p_]
                    maps[i, p_ * bdim : (p_ + 1) * bdim, k * LANES : (k + 1) * LANES] = (
                        jnp.concatenate(
                            [block if q_ == p_ else zero for q_ in range(per)], axis=1
                        )
                    )

    @scoped("norm")
    def norm(read, s, gain):
        step = 128

        def body(i, _):
            r = pl.ds(pl.multiple_of(i * step, step), step)
            total = jnp.zeros((step, 1), f32)
            for b in range(fs):
                v = read(b, r).astype(f32)
                total = total + jnp.sum(v * v, axis=-1, keepdims=True)
            scale = lax.rsqrt(total / (fs * c) + EPS)
            for b in range(fs):
                v = read(b, r).astype(f32)
                nrm[s, b, r, :] = (v * scale * gain[:, b * c : (b + 1) * c]).astype(bf16)
            return 0

        lax.fori_loop(0, length // step, body, 0)

    def tok_block(s):
        return lambda b, r: tok[s, b // hb, r, b % hb * c : (b % hb + 1) * c]

    @scoped("dot")
    def dot(b, s, at, first):
        n = buf[b].shape[2]
        tile = 256
        src = pl.ds(at * ny, ny)
        rows = jnp.concatenate([nrm[s, at * ny + i] for i in range(ny)], axis=1)

        def one(cols):
            v = jnp.dot(
                rows, buf[b][src, :, cols].reshape(ny * c, -1), preferred_element_type=f32
            )
            if first:
                acc[s, :, cols] = v
            else:
                acc[s, :, cols] += v

        def body(i, _):
            one(pl.ds(pl.multiple_of(i * tile, tile), tile))
            return 0

        lax.fori_loop(0, n // tile, body, 0)
        if n % tile:
            one(pl.ds(n // tile * tile, n % tile))

    def from_y(b, d):
        if ny > 1:
            for g, group in enumerate(groups):
                if group[0] == b and not group[3]:
                    p = piece(g, lax.rem(z - d + nz, nz), 1)
                    arrived(copy(p, p, ys.at[g, d], yr.at[g, d], over_y))

    def ready(b, i):
        need(b, i + 1)
        from_y(b, 0 if i < 0 else lax.rem(z - nth(i) + nz, nz))

    def dots(b, s, i):
        run(DOT[b], dot, b, s, z if i < 0 else nth(i), i < 0)

    @scoped("recur")
    def recurrence(s, lo, hi):
        extra = jnp.transpose(ex[s])[:, :1]

        def body(i, _):
            lanes = pl.ds(pl.multiple_of(i * LANES, LANES), LANES)
            glanes = pl.ds(pl.multiple_of(width + i * LANES, LANES), LANES)
            wide = pl.ds(pl.multiple_of(rep * width + i * LANES, LANES), LANES)
            values = (acc[s, :, lanes] * iscale_ref[:, wide]).astype(bf16).astype(f32)
            gate = (acc[s, :, glanes] * gscale_ref[:, wide]).astype(bf16).astype(f32)
            gated[s, :, lanes] = rec_block(
                values, gate, taps_ref[:, wide], maps[i], rates[:, lanes], extra
            )
            return 0

        lax.fori_loop(lo, hi, body, 0)

    def tp_copy(l, s, j):
        return copy(
            thr_s.at[s, j], thr_r.at[s, j], ps.at[l, s, j], pr.at[l, s, j], over_tp
        )

    def x_copy(l, j):
        return copy(xs.at[j], xr.at[j], xss.at[l, j], xrs.at[l, j], over_x)

    @scoped("project")
    def project(l, s, j):
        acts, w = (gated, b1) if l == 0 else (hid, b3)
        theirs = jnp.dot(acts[s], w[(1 - tp) * hb + j], preferred_element_type=f32)
        thr_s[s, j] = theirs.astype(bf16)
        tp_copy(l, s, j).start()
        part[s, j] = jnp.dot(acts[s], w[tp * hb + j], preferred_element_type=f32)

    @scoped("send")
    def send_pair(l, j):
        tp_copy(l, 1, j).wait_recv()
        xs[j] = (part[1, j] + thr_r[1, j].astype(f32)).astype(bf16)
        x_copy(l, j).start()

    def own_scale(ref, j):
        return jnp.where(
            tp == 0, ref[:, j * c : (j + 1) * c], ref[:, (hb + j) * c : (hb + j + 1) * c]
        )

    chunk = max(c, LANES)
    chunks = columns // chunk

    def moved(s, to, q, i, where):
        cols = pl.ds(q * chunk, chunk)
        return copy(
            tok.at[s, tp, :, cols], tok.at[to, tp, :, cols], ms.at[i, q], mr.at[i, q], where
        )

    def m_tp(q):
        return moved(0, 0, q, 0, over_tp)

    def m_x(q):
        return moved(0, 1, q, 1, over_x)

    def m_xtp(q):
        return moved(1, 1, q, 2, over_tp)

    @scoped("mixed")
    def mixed(q):
        for j in range(q * chunk // c, (q + 1) * chunk // c):
            tp_copy(0, 0, j).wait_recv()
            x_copy(0, j).wait_recv()
            total = part[0, j] + thr_r[0, j].astype(f32) + xr[j].astype(f32)
            cols = slice(j * c, (j + 1) * c)
            tok[0, tp, :, cols] = (
                tok[0, tp, :, cols].astype(f32) + total * own_scale(oscale_ref, j)
            ).astype(bf16)
        m_x(q).start()
        m_tp(q).start()

    @scoped("hide")
    def hide(s):
        def silu_up(g, u):
            return (g / (1.0 + jnp.exp(-g)) * u).astype(bf16)

        def body(i, _):
            step = 128
            r = pl.ds(pl.multiple_of(i * step, step), step)
            for k in range(0, main, LANES):
                m = main + k
                g = acc[s, r, k : k + LANES] * guscale[0:1, k : k + LANES]
                u = acc[s, r, m : m + LANES] * guscale[0:1, m : m + LANES]
                hid[s, r, k : k + LANES] = silu_up(g, u)
            if rest:
                both = acc[s, r, 2 * main :] * guscale[0:1, 2 * main :]
                hid[s, r, main:] = silu_up(both, pltpu.roll(both, rest, 1))[:, :rest]
            return 0

        lax.fori_loop(0, length // 128, body, 0)

    def store(q):
        cols = pl.ds(q * chunk, chunk)
        return pltpu.make_async_copy(tok.at[0, tp, :, cols], o_ref.at[:, cols], lsem.at[q])

    @scoped("finish")
    def finish(q):
        m_tp(q).wait_send()
        m_x(q).wait_send()
        for j in range(q * chunk // c, (q + 1) * chunk // c):
            tp_copy(1, 0, j).wait_recv()
            x_copy(1, j).wait_recv()
            total = part[0, j] + thr_r[0, j].astype(f32) + xr[j].astype(f32)
            cols = slice(j * c, (j + 1) * c)
            tok[0, tp, :, cols] = (
                tok[0, tp, :, cols].astype(f32) + total * own_scale(dscale_ref, j)
            ).astype(bf16)
        store(q).start()

    ranks = range(-1, nz - 1)
    blocks = width // LANES
    spans = [(lo, min(lo + 2, blocks)) for lo in range(0, blocks, 2)]
    wait_until(6.0, arrived, tok_tp)
    run(1.3, norm, tok_block(0), 0, mgain_ref)
    run(1.4, pack)
    run(1.0, tables)
    ready(0, -1)
    dots(0, 0, -1)
    wait_until(27.0, arrived, tok_x)
    tok_xtp.start()
    wait_until(31.0, arrived, tok_xtp)
    run(1.3, norm, tok_block(1), 1, mgain_ref)
    for sent in (tok_tp, tok_x, tok_xtp, extra_x):
        sent.wait_send()
    dots(0, 1, -1)
    for i in ranks[1:]:
        ready(0, i)
        for s in (0, 1):
            dots(0, s, i)
    arrived(extra_x)
    for s in (1, 0):
        for span in spans:
            run(3.3, recurrence, s, *span)
    for i in ranks:
        ready(1, i)
    for j in range(hb):
        run(0.9, project, 0, 1, j)
        if j:
            run(0.3, send_pair, 0, j - 1)
    run(0.3, send_pair, 0, hb - 1)
    start = clock[0]
    for j in range(hb):
        run(0.9, project, 0, 0, j)
    hop = HOP / chunks
    for q in range(chunks):
        wait_until(start + (q + 0.8) * hop, mixed, q)
    for q in range(chunks):
        arrived(m_tp(q))
    run(1.3, norm, tok_block(0), 0, fgain_ref)
    start += (chunks + 0.2) * hop
    ready(2, -1)
    dots(2, 0, -1)
    for q in range(chunks):
        wait_until(start + (q + 1) * hop, arrived, m_x(q))
        m_xtp(q).start()
    for q in range(chunks):
        arrived(m_xtp(q))
    run(1.3, norm, tok_block(1), 1, fgain_ref)
    dots(2, 1, -1)
    for i in ranks[1:]:
        ready(2, i)
        for s in (1, 0):
            dots(2, s, i)
    run(0.8, hide, 1)
    run(0.8, hide, 0)
    for j in range(hb):
        x_copy(0, j).wait_send()
        for s in range(2):
            tp_copy(0, s, j).wait_send()

    need(3, half)
    for w in (0, 1) if ny > 1 else (0,):
        for k in range(half):
            if w:
                from_y(3, k)
                from_y(3, k + half)
            else:
                need(3, half if k == 0 else nz - 1)
            j = lax.rem(z - k + nz, half) * ny + (1 - y if w else y)
            run(0.55, project, 1, 1, j)
            run(0.55, project, 1, 0, j)
            run(0.3, send_pair, 1, j)
    for q in range(chunks):
        finish(q)

    for g, group in enumerate(groups):
        for k in range(1, nz):
            for w in tracks(g):

                @pl.when(can_up(k))
                def _():
                    up(g, w, k, z - k + 1).wait_send()

                @pl.when(can_down(k))
                def _():
                    down_z(g, w, k, z + k - 1).wait_send()

        if ny > 1:
            for d in [0] if group[3] else range(nz):
                over(g, d).wait_send()
    for j in range(hb):
        x_copy(1, j).wait_send()
        for s in range(2):
            tp_copy(1, s, j).wait_send()
    for q in range(chunks):
        m_xtp(q).wait_send()
        store(q).wait()


def layer(ny, nz, tokens, lru_input, lru_gate, lru_output, ffn_gate, ffn_up, ffn_down, *rest):
    fs = ny * nz
    length, columns = tokens.shape
    c = lru_input.shape[0]
    hb = columns // c
    width, hidden = lru_output.shape[0] // 2, ffn_down.shape[0] // 2
    bf16, f32 = jnp.bfloat16, jnp.float32
    dma = pltpu.SemaphoreType.DMA
    vmem = pl.BlockSpec(memory_space=pltpu.VMEM)
    hbm = pl.BlockSpec(memory_space=pl.ANY)
    return pl.pallas_call(
        functools.partial(layer_kernel, ny, nz),
        out_shape=jax.ShapeDtypeStruct((length, columns), bf16),
        in_specs=[hbm] * 7 + [vmem] * len(rest),
        out_specs=hbm,
        scratch_shapes=[
            pltpu.VMEM((2, 2, length, columns), bf16),
            pltpu.VMEM((2, 8, length), f32),
            pltpu.VMEM((2, fs, length, c), bf16),
            pltpu.VMEM((fs, c, 2 * width), bf16),
            pltpu.VMEM((fs, width, c), bf16),
            pltpu.VMEM((fs, c, 2 * hidden), bf16),
            pltpu.VMEM((fs, hidden, c), bf16),
            pltpu.VMEM((2, c, width), f32),
            pltpu.VMEM((width, c), f32),
            pltpu.VMEM((hidden, c), f32),
            pltpu.VMEM((2, length, 2 * max(width, hidden)), f32),
            pltpu.VMEM((2, length, width), bf16),
            pltpu.VMEM((2, length, hidden), bf16),
            pltpu.VMEM((2, hb, length, c), f32),
            pltpu.VMEM((2, hb, length, c), bf16),
            pltpu.VMEM((2, hb, length, c), bf16),
            pltpu.VMEM((hb, length, c), bf16),
            pltpu.VMEM((hb, length, c), bf16),
            pltpu.VMEM((width // LANES, LANES, 2 * LANES), f32),
            pltpu.VMEM((1, width), f32),
            pltpu.VMEM((8, 2 * hidden), f32),
            dma((max(7, columns // max(c, LANES)),)),
            dma((9, 2, nz)),
            dma((9, 2, nz)),
            dma((9, 2, nz)),
            dma((9, 2, nz)),
            dma((9, nz)),
            dma((9, nz)),
            dma((4,)),
            dma((4,)),
            dma((2, 2, hb)),
            dma((2, 2, hb)),
            dma((2, hb)),
            dma((2, hb)),
            dma((3, hb)),
            dma((3, hb)),
        ],
        compiler_params=pltpu.CompilerParams(
            collective_id=0, has_side_effects=True, vmem_limit_bytes=67_000_000
        ),
        name="layer",
    )(tokens, lru_input, lru_gate, lru_output, ffn_gate, ffn_up, ffn_down, *rest)


def local(mesh_fs, *args):
    (
        tokens,
        mix_gain,
        lru_input,
        lru_gate,
        lru_input_scale,
        lru_gate_scale,
        conv_weight,
        recur_gate,
        input_gate,
        decay_rate,
        extra_decay,
        lru_output,
        lru_output_scale,
        ffn_gain,
        ffn_gate,
        ffn_up,
        ffn_gate_scale,
        ffn_up_scale,
        ffn_down,
        ffn_down_scale,
    ) = args
    ny = 2 if mesh_fs % 2 == 0 else 1
    return layer(
        ny,
        mesh_fs // ny,
        tokens,
        lru_input,
        lru_gate,
        lru_output,
        ffn_gate,
        ffn_up,
        ffn_down,
        extra_decay[None, :],
        mix_gain[None, :],
        ffn_gain[None, :],
        lru_input_scale[None, :],
        lru_gate_scale[None, :],
        lru_output_scale[None, :],
        jnp.stack([ffn_gate_scale, ffn_up_scale]),
        ffn_down_scale[None, :],
        conv_weight,
        recur_gate,
        input_gate,
        decay_rate[None, :],
    )


def solution(mesh):
    in_specs = (
        P(("rep", "fs"), "tp"),
        P(),
        P("fs", "tp"),
        P("fs", "tp"),
        P("tp"),
        P("tp"),
        P(None, "tp"),
        P("tp", None, None),
        P("tp", None, None),
        P("tp"),
        P(("rep", "fs")),
        P("tp", "fs"),
        P(),
        P(),
        P("fs", "tp"),
        P("fs", "tp"),
        P("tp"),
        P("tp"),
        P("tp", "fs"),
        P(),
    )
    out_specs = P(("rep", "fs"), "tp")
    mesh_fs = mesh.shape["fs"]
    return jax.shard_map(
        lambda *args: local(mesh_fs, *args),
        mesh=mesh,
        in_specs=in_specs,
        out_specs=out_specs,
        check_vma=False,
    )
```

profile of v0, /device:TPU:0, one launch (start us, length us, event | category | flops | bytes accessed | tf_op | source)
XLA Modules:
  0.0 199.8 jit_solution(16745298394747523475)
XLA Ops:
  0.0 0.7 stack.9
  0.7 0.7 stack.10
  1.4 0.6 pad_maximum_fusion.fscale_ref
  2.0 195.6 %layer.1 = bf16[512,1024]{1,0:T(8,128)(2,1)} custom-call(bf16[512,1024]{1,0:T(8,128)(2,1)} %tokens.1, f32[256,1024]{1,0:T(8,128)} %lru_input.1, f32[256,1024]{1,0:T(8,128)} %lru_gate.1, f32[1024,256]{1,0:T(8,128)} %lru_output.1, f32[256,1408]{1,0:T(8,128)} %ffn_gate.1, f32[256,1408]{1,0:T(8,128)} %ffn_up.1, f32[1408,256]{1,0:T(8,128)} %ffn_down.1, ...), custom_call_target="tpu_custom_call" | custom-call | tf_op jit(solution)/shard_map/layer/pallas_call | solution.py:695
  197.6 2.3 %copy.22 = bf16[512,1024]{1,0:T(8,128)(2,1)} copy(bf16[512,1024]{1,0:T(8,128)(2,1)} %layer.1) | data formatting | bytes 2097152
where the time goes:
time: 200 us
  Pallas kernels  196 us (98%)
  local copies, waits for them, and re-layouts  3.66 us (2%)
    pallas_call x1, Pallas kernels, layer(): pl.pallas_call(functools.partial(layer_kernel, ny, nz), out_shape=jax.Sha...  196 us

commit v1 on v0

v1 whole, which is shorter than its diff:
```python
import functools

import jax
import jax.numpy as jnp
from jax import lax
from jax.experimental import pallas as pl
from jax.experimental.pallas import tpu as pltpu
from jax.sharding import PartitionSpec as P

EPS = 1e-06
RATE = 8.0
LANES = 128
FIRST = 9.0
RATE_BOTH = 21500.0
EARLY = 4
TOKENS = 39.0
HOP = 22.5
DOT = (1.5, 0.0, 2.2)
MESH = pl.DeviceIdType.MESH


def scoped(name):
    def wrap(f):
        def inner(*args):
            with jax.named_scope(name + "".join(f"_{a}" for a in args if isinstance(a, int))):
                return f(*args)

        return inner

    return wrap


def sigmoid(v):
    return 1.0 / (1.0 + jnp.exp(-v))


def rec_block(values, gate, taps, maps, rate, extra):
    length = values.shape[0]
    ntaps = taps.shape[0]
    row = lax.broadcasted_iota(jnp.int32, values.shape, 0)
    conv = taps[ntaps - 1 : ntaps, :] * values
    for back in range(1, ntaps):
        moved = jnp.where(row >= back, pltpu.roll(values, back, 0), 0.0)
        conv = conv + taps[ntaps - 1 - back : ntaps - back, :] * moved
    mapped = jnp.dot(
        conv, maps, preferred_element_type=jnp.float32, precision=lax.Precision.HIGHEST
    )
    recur = sigmoid(mapped[:, :LANES])
    ingate = sigmoid(mapped[:, LANES:])
    log_rate = rate * recur - extra
    a = jnp.exp(log_rate)
    u = -2.0 * log_rate
    series = u * (1 - u / 2 * (1 - u / 3 * (1 - u / 4 * (1 - u / 5 * (1 - u / 6)))))
    b = jnp.sqrt(jnp.where(u < 0.25, series, 1.0 - jnp.exp(-u))) * (ingate * conv)
    inner = row % 8
    for s in (1, 2, 4):
        keep = inner >= s
        b = jnp.where(keep, a * pltpu.roll(b, s, 0) + b, b)
        a = jnp.where(keep, a * pltpu.roll(a, s, 0), a)
    groups = length // 8
    last_a = a.reshape(groups, 8, LANES)
    last_b = b.reshape(groups, 8, LANES)
    ca = jnp.broadcast_to(last_a[:, 7:8, :], last_a.shape).reshape(length, LANES)
    cb = jnp.broadcast_to(last_b[:, 7:8, :], last_b.shape).reshape(length, LANES)
    s = 8
    while s < length:
        cb_new = ca[s:] * cb[:-s] + cb[s:]
        ca_new = ca[s:] * ca[:-s]
        cb = jnp.concatenate([cb[:s], cb_new], axis=0)
        ca = jnp.concatenate([ca[:s], ca_new], axis=0)
        s *= 2
    state = jnp.concatenate([b[:8], a[8:] * cb[:-8] + b[8:]], axis=0)
    gelu = 0.5 * gate * (1.0 + jnp.tanh(0.7978845608028654 * (gate + 0.044715 * gate * gate * gate)))
    return (state * gelu).astype(jnp.bfloat16)


def layer_kernel(
    ny,
    nz,
    tokens,
    lru_input,
    lru_gate,
    lru_output,
    ffn_gate,
    ffn_up,
    ffn_down,
    extra_ref,
    mgain_ref,
    fgain_ref,
    iscale_ref,
    gscale_ref,
    oscale_ref,
    fscale_ref,
    dscale_ref,
    taps_ref,
    rmap_ref,
    imap_ref,
    decay_ref,
    o_ref,
    tok,
    ex,
    nrm,
    b0,
    b1,
    b2,
    b3,
    give_mix,
    give_out,
    give_gu,
    give_down,
    acc,
    gated,
    hid,
    part,
    thr_s,
    thr_r,
    xr,
    maps,
    rates,
    guscale,
    lsem,
    us,
    ur,
    ds,
    dr,
    ys,
    yr,
    ts,
    tr,
    ps,
    pr,
    xss,
    xrs,
    ms,
    mr,
    free,
):
    f32, bf16 = jnp.float32, jnp.bfloat16
    fs = ny * nz
    length, columns = tokens.shape
    c = lru_input.shape[0]
    hb = columns // c
    width = gated.shape[2]
    hidden = hid.shape[2]
    rep, tp, me = lax.axis_index("rep"), lax.axis_index("tp"), lax.axis_index("fs")
    z, y = me // ny, me % ny
    buf = (b0, b1, b2, b3)
    twin = {"rep": 1 - rep}
    over_tp = {"tp": 1 - tp}
    pair = {"fs": z * ny + (1 - y)}
    give = (give_mix, give_out, give_gu, give_down)
    half = nz // 2
    plan = ((64, 96, 96), (256, 256), (96, 96, 64))
    groups = []
    for b, parts in enumerate(plan):
        row, rows = 0, buf[b].shape[1]
        for i, n in enumerate(parts):
            n = rows - row if i + 1 == len(parts) else max(16, n * rows // sum(parts) // 16 * 16)
            groups.append((b, row, n))
            row += n
    subs = b3.shape[1]
    cs = c // subs
    groups += [(3, i, hidden) for i in range(subs)]

    clock = [0.0]
    eta, slots, at_time = {}, [], FIRST
    for g, (b, _, n) in enumerate(groups):
        size = n * buf[b].shape[-1]
        for k in range(1, nz):
            at_time += size / RATE_BOTH
            eta[g, k] = at_time
            slots.append((g, k))

    def copy(src, dst, s, r, where):
        return pltpu.make_async_remote_copy(
            src_ref=src, dst_ref=dst, send_sem=s, recv_sem=r, device_id=where, device_id_type=MESH
        )

    def cut(g, ref, *at):
        b, row, rows = groups[g]
        return ref.at[(*at, row if b == 3 else pl.ds(row, rows))]

    def piece(g, at, w):
        return cut(g, buf[groups[g][0]], at * ny + (rep if w == 0 else 1 - rep))

    def up(g, k, at):
        p = piece(g, at, 0)
        return copy(p, p, us.at[g, k], ur.at[g, k], {"fs": lax.rem(z + 1, nz) * ny + y})

    def down_z(g, k, at):
        p = piece(g, at, 0)
        return copy(p, p, ds.at[g, k], dr.at[g, k], {"fs": lax.rem(z + nz - 1, nz) * ny + y})

    def from_z(d):
        return lax.rem(z - d + nz, nz)

    def over(g, d, w=0):
        p = piece(g, from_z(d), w)
        return copy(p, p, ys.at[g, d], yr.at[g, d], twin)

    def swap(g):
        b = groups[g][0]
        return copy(cut(g, give[b]), cut(g, buf[b], me), ys.at[g, 0], yr.at[g, 0], pair)

    def can_up(k):
        return (z + 1 < nz) & (z >= k - 1)

    def can_down(k):
        return (z > 0) & (z + k <= nz)

    def own_y(g):
        if g < len(groups):
            swap(g).start()

    def own_z(g):
        if g < len(groups):
            swap(g).wait_recv()

            @pl.when(can_up(1))
            def _():
                up(g, 1, z).start()

            @pl.when(can_down(1))
            def _():
                down_z(g, 1, z).start()

    @scoped("slot")
    def slot(g, k):
        if k == nz - 1 and g <= EARLY:
            own_z(g + 1)
            for n in {2: (5, 6), 3: (7,), 4: (8, 9)}.get(g, ()):
                own_y(n)
            if g == EARLY:
                own_z(g + 2)
        if k == 1 and g > EARLY:
            own_z(g + 2)

        @pl.when(z >= k)
        def _():
            up(g, k, z - k).wait_recv()
            if k + 1 < nz:

                @pl.when(can_up(k + 1))
                def _():
                    up(g, k + 1, z - k).start()

            over(g, k).start()

        @pl.when(z + k < nz)
        def _():
            down_z(g, k, z + k).wait_recv()
            if k + 1 < nz:

                @pl.when(can_down(k + 1))
                def _():
                    down_z(g, k + 1, z + k).start()

            over(g, nz - k).start()

    def next_slot():
        key = slots.pop(0)
        clock[0] = max(clock[0], eta[key])
        slot(*key)

    def pump(until):
        while slots and eta[slots[0]] <= until:
            next_slot()

    def need(b, k):
        g = max(i for i, group in enumerate(groups) if group[0] == b)
        while slots and slots[0] <= (g, k):
            next_slot()

    def run(cost, f, *args):
        pump(clock[0] + cost / 2)
        f(*args)
        clock[0] += cost

    def wait_until(when, f, *args):
        pump(when)
        f(*args)
        clock[0] = max(clock[0], when)

    def nth(i):
        near = jnp.minimum(z, nz - 1 - z)
        step = i // 2 + 1
        both = z - step if i % 2 == 0 else z + step
        far = i - near + 1
        rest = jnp.where(z > nz - 1 - z, z - far, z + far)
        return jnp.where(i < 2 * near, both, rest)

    def stage(src, dst, i):
        return pltpu.make_async_copy(src, dst, lsem.at[i])

    mine_cols = pl.ds(pl.multiple_of(y * width, LANES), width)
    give_cols = pl.ds(pl.multiple_of((1 - y) * width, LANES), width)
    cuts = range(0, hidden, length)
    loads = [
        stage(lru_input, acc.at[0, c : 2 * c, : 2 * width], 0),
        stage(lru_gate, acc.at[1, c : 2 * c, : 2 * width], 1),
        stage(tokens, tok.at[0, tp], 2),
        stage(ffn_gate, acc.at[0, :c], 3),
        stage(ffn_up, acc.at[1, :c], 4),
    ]
    for h in range(2):
        for i in range(subs):
            cols = pl.ds(i * cs, cs)
            src = lru_output.at[pl.ds(h * width, width), cols]
            loads.append(stage(src, part.at[0, h * subs + i, :width], len(loads)))
    for h in range(2):
        for i in range(subs):
            for r, row in enumerate(cuts):
                n = min(length, hidden - row)
                src = ffn_down.at[pl.ds(h * hidden + row, n), pl.ds(i * cs, cs)]
                to = part.at[1, (h * subs + i) * len(cuts) + r, :n]
                loads.append(stage(src, to, len(loads)))
    for load in loads:
        load.start()

    barrier = pltpu.get_barrier_semaphore()

    def greet(where):
        pl.semaphore_signal(barrier, inc=1, device_id=where, device_id_type=MESH)

    greet(pair)
    greet(twin)
    greet(over_tp)
    pl.when(z + 1 < nz)(lambda: greet({"fs": lax.rem(z + 1, nz) * ny + y}))
    pl.when(z > 0)(lambda: greet({"fs": lax.rem(z + nz - 1, nz) * ny + y}))

    loads[0].wait()
    loads[1].wait()
    for i in range(2):
        cols = slice(i * width, (i + 1) * width)
        give_mix[:, cols] = acc[i, c : 2 * c, give_cols].astype(bf16)
        b0[me, :, cols] = acc[i, c : 2 * c, mine_cols].astype(bf16)
    ex[0] = jnp.broadcast_to(extra_ref[...], ex.shape[1:])
    loads[2].wait()

    along_z = jnp.where(z > 0, 1, 0) + jnp.where(z + 1 < nz, 1, 0)
    pl.semaphore_wait(barrier, 3 + along_z)

    def tok_copy(s, i, where, to):
        return copy(tok.at[s, tp], tok.at[to, tp], ts.at[i], tr.at[i], where)

    tok_tp = tok_copy(0, 0, over_tp, 0)
    tok_x = tok_copy(0, 1, pair, 1)
    tok_xtp = tok_copy(1, 2, over_tp, 1)
    extra_x = copy(ex.at[0], ex.at[1], ts.at[3], tr.at[3], pair)
    own_y(0)
    tok_tp.start()
    extra_x.start()
    for load in loads[5 : 5 + 2 * subs]:
        load.wait()
    for i in range(subs):
        cols = slice(i * cs, (i + 1) * cs)
        b1[me, :, cols] = part[0, y * subs + i, :width].astype(bf16)
        give_out[:, cols] = part[0, (1 - y) * subs + i, :width].astype(bf16)
    own_y(1)
    own_y(2)
    own_z(0)

    @scoped("wait")
    def arrived(c):
        c.wait_recv()

    main = hidden // LANES * LANES
    rest = hidden - main

    @scoped("pack")
    def pack():
        loads[3].wait()
        loads[4].wait()
        step = 32

        def half_of(v, which):
            return jnp.where(which == 0, v, pltpu.roll(v, hidden, 1))

        def joined(g, u, which):
            g, u = half_of(g, which), half_of(u, which)
            out = [g[:, :main], u[:, :main]]
            if rest:
                g, u = g[:, main : main + LANES], u[:, main : main + LANES]
                lane = lax.broadcasted_iota(jnp.int32, g.shape, 1)
                out.append(jnp.where(lane < rest, g, pltpu.roll(u, rest, 1)))
            return out

        def body(i, _):
            r = pl.ds(pl.multiple_of(i * step, step), step)
            for which, to in ((y, b2.at[me]), (1 - y, give_gu)):
                out = joined(acc[0, r, :], acc[1, r, :], which)
                to[r, :main] = out[0].astype(bf16)
                to[r, main : 2 * main] = out[1].astype(bf16)
                if rest:
                    to[r, 2 * main :] = out[2].astype(bf16)
            return 0

        lax.fori_loop(0, c // step, body, 0)
        wide = (8, 2 * hidden)
        out = joined(
            jnp.broadcast_to(fscale_ref[0:1, :], wide),
            jnp.broadcast_to(fscale_ref[1:2, :], wide),
            y,
        )
        guscale[:, :main] = out[0]
        guscale[:, main : 2 * main] = out[1]
        if rest:
            guscale[:, 2 * main :] = out[2]
        for load in loads[5 + 2 * subs :]:
            load.wait()
        for i in range(subs):
            for which, to in ((y, b3.at[me, i]), (1 - y, give_down.at[i])):
                for r, row in enumerate(cuts):
                    n = min(length, hidden - row)
                    at = (which * subs + i) * len(cuts) + r
                    to[row : row + n] = part[1, at, :n].astype(bf16)

    @scoped("tables")
    def tables():
        v = -decay_ref[:, mine_cols]
        e = jnp.exp(-jnp.abs(v))
        q = e / (2.0 + e)
        p = q * q
        poly = jnp.full_like(p, 1.0 / 17)
        for odd in range(15, 0, -2):
            poly = poly * p + 1.0 / odd
        rates[...] = -RATE * (jnp.maximum(v, 0.0) + 2.0 * q * poly)
        bdim = rmap_ref.shape[1]
        per = LANES // bdim
        zero = jnp.zeros((bdim, bdim), f32)
        for i in range(width // LANES):
            for p_ in range(per):
                for k, ref in enumerate((rmap_ref, imap_ref)):
                    block = ref[y * (width // bdim) + i * per + p_]
                    maps[i, p_ * bdim : (p_ + 1) * bdim, k * LANES : (k + 1) * LANES] = (
                        jnp.concatenate(
                            [block if q_ == p_ else zero for q_ in range(per)], axis=1
                        )
                    )

    @scoped("norm")
    def norm(read, s, gain):
        step = 128

        def body(i, _):
            r = pl.ds(pl.multiple_of(i * step, step), step)
            total = jnp.zeros((step, 1), f32)
            for b in range(fs):
                v = read(b, r).astype(f32)
                total = total + jnp.sum(v * v, axis=-1, keepdims=True)
            scale = lax.rsqrt(total / (fs * c) + EPS)
            for b in range(fs):
                v = read(b, r).astype(f32)
                nrm[s, b, r, :] = (v * scale * gain[:, b * c : (b + 1) * c]).astype(bf16)
            return 0

        lax.fori_loop(0, length // step, body, 0)

    def tok_block(s):
        return lambda b, r: tok[s, b // hb, r, b % hb * c : (b % hb + 1) * c]

    @scoped("dot")
    def dot(b, s, at, first):
        n = buf[b].shape[2]
        tile = 256
        src = pl.ds(at * ny, ny)
        rows = jnp.concatenate([nrm[s, at * ny + i] for i in range(ny)], axis=1)

        def one(cols):
            v = jnp.dot(
                rows, buf[b][src, :, cols].reshape(ny * c, -1), preferred_element_type=f32
            )
            if first:
                acc[s, :, cols] = v
            else:
                acc[s, :, cols] += v

        def body(i, _):
            one(pl.ds(pl.multiple_of(i * tile, tile), tile))
            return 0

        lax.fori_loop(0, n // tile, body, 0)
        if n % tile:
            one(pl.ds(n // tile * tile, n % tile))

    def from_twin(b, d, sub=0):
        for g, group in enumerate(groups):
            if group[0] == b and (b < 3 or group[1] == sub):
                arrived(over(g, d, 1))

    def ready(b, i):
        need(b, i + 1)
        if i >= 0:
            from_twin(b, lax.rem(z - nth(i) + nz, nz))

    def dots(b, s, i):
        run(DOT[b], dot, b, s, z if i < 0 else nth(i), i < 0)

    @scoped("recur")
    def recurrence(s, lo, hi):
        extra = jnp.transpose(ex[s])[:, :1]

        def body(i, _):
            lanes = pl.ds(pl.multiple_of(i * LANES, LANES), LANES)
            glanes = pl.ds(pl.multiple_of(width + i * LANES, LANES), LANES)
            wide = pl.ds(pl.multiple_of(y * width + i * LANES, LANES), LANES)
            values = (acc[s, :, lanes] * iscale_ref[:, wide]).astype(bf16).astype(f32)
            gate = (acc[s, :, glanes] * gscale_ref[:, wide]).astype(bf16).astype(f32)
            gated[s, :, lanes] = rec_block(
                values, gate, taps_ref[:, wide], maps[i], rates[:, lanes], extra
            )
            return 0

        lax.fori_loop(lo, hi, body, 0)

    def part_of(j, i):
        return pl.ds(j * subs, subs) if i is None else pl.ds(j * subs + i, 1)

    def tp_copy(l, s, j, i=None):
        at, sem = part_of(j, i), j * subs + (i or 0)
        return copy(thr_s.at[s, at], thr_r.at[s, at], ps.at[l, s, sem], pr.at[l, s, sem], over_tp)

    def x_copy(l, s, j, i=None):
        at, sem = part_of(j, i), j * subs + (i or 0)
        return copy(
            thr_s.at[s, at], xr.at[1 - s, at], xss.at[l, s, sem], xrs.at[l, 1 - s, sem], pair
        )

    def x_arrived(l, s, j, i=None):
        x_copy(l, 1 - s, j, i).wait_recv()

    @scoped("project")
    def project(l, s, j, i=None):
        theirs, mine = (1 - tp) * hb + j, tp * hb + j

        def product(at):
            acts, w = (gated, b1.at[at]) if l == 0 else (hid, b3.at[at, i])
            return jnp.dot(acts[s], w[...], preferred_element_type=f32)

        def put(to, v):
            for k in range(subs) if i is None else (i,):
                cols = slice(k * cs, (k + 1) * cs) if i is None else slice(0, cs)
                to[s, j * subs + k] = v[:, cols].astype(to.dtype)

        put(thr_s, product(theirs))
        tp_copy(l, s, j, i).start()
        put(part, product(mine))

    @scoped("send")
    def send(l, s, j, i=None):
        tp_copy(l, s, j, i).wait()
        at = part_of(j, i)
        total = part[s, at] + thr_r[s, at].astype(f32)
        thr_s[s, at] = total.astype(bf16)
        x_copy(l, s, j, i).start()
        if l == 0:
            part[s, at] = total

    def residual(scale, s, j, k):
        at = j * subs + k
        total = part[s, at] + xr[s, at].astype(f32)
        if scale is dscale_ref:
            total = total + thr_r[s, at].astype(f32)
        lo = j * c + k * cs
        cols = slice(lo, lo + cs)
        factor = jnp.where(
            tp == 0, scale[:, cols], scale[:, columns + lo : columns + lo + cs]
        )
        tok[s, tp, :, cols] = (tok[s, tp, :, cols].astype(f32) + total * factor).astype(bf16)

    chunk = max(c, LANES)
    chunks = columns // chunk

    def m_tp(s, q):
        at = tok.at[s, tp, :, pl.ds(q * chunk, chunk)]
        return copy(at, at, ms.at[s, q], mr.at[s, q], over_tp)

    @scoped("mixed")
    def mixed(s, q):
        for j in range(q * chunk // c, (q + 1) * chunk // c):
            x_arrived(0, s, j)
            for k in range(subs):
                residual(oscale_ref, s, j, k)
        m_tp(s, q).start()

    @scoped("hide")
    def hide(s):
        def silu_up(g, u):
            return (g / (1.0 + jnp.exp(-g)) * u).astype(bf16)

        def body(i, _):
            step = 128
            r = pl.ds(pl.multiple_of(i * step, step), step)
            for k in range(0, main, LANES):
                m = main + k
                g = acc[s, r, k : k + LANES] * guscale[0:1, k : k + LANES]
                u = acc[s, r, m : m + LANES] * guscale[0:1, m : m + LANES]
                hid[s, r, k : k + LANES] = silu_up(g, u)
            if rest:
                both = acc[s, r, 2 * main :] * guscale[0:1, 2 * main :]
                hid[s, r, main:] = silu_up(both, pltpu.roll(both, rest, 1))[:, :rest]
            return 0

        lax.fori_loop(0, length // 128, body, 0)

    def store(q):
        cols = pl.ds(q * chunk, chunk)
        return pltpu.make_async_copy(tok.at[0, tp, :, cols], o_ref.at[:, cols], lsem.at[q])

    @scoped("finish")
    def finish(q):
        m_tp(0, q).wait_send()
        for j in range(q * chunk // c, (q + 1) * chunk // c):
            for k in range(subs):
                tp_copy(1, 0, j, k).wait_recv()
                x_arrived(1, 0, j, k)
                residual(dscale_ref, 0, j, k)
        store(q).start()

    ranks = range(-1, nz - 1)
    blocks = width // LANES
    spans = [(lo, min(lo + 2, blocks)) for lo in range(0, blocks, 2)]
    wait_until(6.0, arrived, tok_tp)
    run(1.3, norm, tok_block(0), 0, mgain_ref)
    next_slot()
    tok_x.start()
    run(1.4, pack)
    run(1.0, tables)
    wait_until(TOKENS, arrived, tok_x)
    tok_xtp.start()
    own_y(3)
    own_y(4)
    wait_until(TOKENS + 3.0, arrived, tok_xtp)
    run(1.3, norm, tok_block(1), 1, mgain_ref)
    for sent in (tok_tp, tok_x, tok_xtp, extra_x):
        sent.wait_send()
    ready(0, -1)
    for s in (0, 1):
        dots(0, s, -1)
    for i in ranks[1:]:
        ready(0, i)
        for s in (0, 1):
            dots(0, s, i)
    arrived(extra_x)
    for s in (1, 0):
        for span in spans:
            run(3.3, recurrence, s, *span)
    for i in ranks:
        ready(1, i)
    for s in (1, 0):
        for j in range(hb):
            run(0.9, project, 0, s, j)
            if j:
                run(0.4, send, 0, s, j - 1)
        run(0.4, send, 0, s, hb - 1)
    start = clock[0] - 8
    for s in (0, 1):
        for q in range(chunks):
            wait_until(start + HOP * (s + (q + 1) / chunks), mixed, s, q)
        if s == 0:
            pl.semaphore_signal(free, inc=1, device_id=pair, device_id_type=MESH)
        else:
            ready(2, -1)
            dots(2, 0, -1)
        for q in range(chunks):
            arrived(m_tp(s, q))
        run(1.3, norm, tok_block(s), s, fgain_ref)
    dots(2, 1, -1)
    for i in ranks[1:]:
        ready(2, i)
        for s in (1, 0):
            dots(2, s, i)
    run(0.8, hide, 1)
    run(0.8, hide, 0)
    for j in range(hb):
        for s in range(2):
            x_copy(0, s, j).wait_send()
    pl.semaphore_wait(free, 1)

    for i in range(subs):
        g = len(groups) - subs + i
        for w in (0, 1):
            for k in range(half):
                d = half if k == 0 and w == 0 else nz - 1
                while slots and slots[0] <= (g, d):
                    next_slot()
                if w:
                    if k:
                        from_twin(3, k, i)
                    from_twin(3, k + half, i)
                j = lax.rem(z - k + nz, half) * ny + (1 - rep if w else rep)
                run(0.4, project, 1, 1, j, i)
                run(0.4, project, 1, 0, j, i)
                run(0.3, send, 1, 1, j, i)
    for q in range(chunks):
        finish(q)

    @scoped("sent")
    def sent_all():
        for g in range(len(groups)):
            for k in range(1, nz):

                @pl.when(can_up(k))
                def _():
                    up(g, k, z - k + 1).wait_send()

                @pl.when(can_down(k))
                def _():
                    down_z(g, k, z + k - 1).wait_send()

                over(g, k).wait_send()
            swap(g).wait_send()
        for j in range(hb):
            for i in range(subs):
                x_copy(1, 1, j, i).wait_send()
                tp_copy(1, 0, j, i).wait_send()
        for q in range(chunks):
            m_tp(1, q).wait_send()

    @scoped("stored")
    def stored():
        for q in range(chunks):
            store(q).wait()

    sent_all()
    stored()


def layer(ny, nz, tokens, lru_input, lru_gate, lru_output, ffn_gate, ffn_up, ffn_down, *rest):
    fs = ny * nz
    length, columns = tokens.shape
    c = lru_input.shape[0]
    hb = columns // c
    width, hidden = lru_output.shape[0] // 2, ffn_down.shape[0] // 2
    subs = 2 if c % (2 * LANES) == 0 else 1
    cut = (hb * subs, length, c // subs)
    bf16, f32 = jnp.bfloat16, jnp.float32
    dma = pltpu.SemaphoreType.DMA
    vmem = pl.BlockSpec(memory_space=pltpu.VMEM)
    hbm = pl.BlockSpec(memory_space=pl.ANY)
    return pl.pallas_call(
        functools.partial(layer_kernel, ny, nz),
        out_shape=jax.ShapeDtypeStruct((length, columns), bf16),
        in_specs=[hbm] * 7 + [vmem] * len(rest),
        out_specs=hbm,
        scratch_shapes=[
            pltpu.VMEM((2, 2, length, columns), bf16),
            pltpu.VMEM((2, 8, length), f32),
            pltpu.VMEM((2, fs, length, c), bf16),
            pltpu.VMEM((fs, c, 2 * width), bf16),
            pltpu.VMEM((fs, width, c), bf16),
            pltpu.VMEM((fs, c, 2 * hidden), bf16),
            pltpu.VMEM((fs, subs, hidden, c // subs), bf16),
            pltpu.VMEM((c, 2 * width), bf16),
            pltpu.VMEM((width, c), bf16),
            pltpu.VMEM((c, 2 * hidden), bf16),
            pltpu.VMEM((subs, hidden, c // subs), bf16),
            pltpu.VMEM((2, length, 2 * max(width, hidden)), f32),
            pltpu.VMEM((2, length, width), bf16),
            pltpu.VMEM((2, length, hidden), bf16),
            pltpu.VMEM((2, *cut), f32),
            pltpu.VMEM((2, *cut), bf16),
            pltpu.VMEM((2, *cut), bf16),
            pltpu.VMEM((2, *cut), bf16),
            pltpu.VMEM((width // LANES, LANES, 2 * LANES), f32),
            pltpu.VMEM((1, width), f32),
            pltpu.VMEM((8, 2 * hidden), f32),
            dma((max(32, columns // LANES),)),
            dma((10, nz)),
            dma((10, nz)),
            dma((10, nz)),
            dma((10, nz)),
            dma((10, nz)),
            dma((10, nz)),
            dma((4,)),
            dma((4,)),
            dma((2, 2, cut[0])),
            dma((2, 2, cut[0])),
            dma((2, 2, cut[0])),
            dma((2, 2, cut[0])),
            dma((2, hb)),
            dma((2, hb)),
            pltpu.SemaphoreType.REGULAR,
        ],
        compiler_params=pltpu.CompilerParams(
            collective_id=0, has_side_effects=True, vmem_limit_bytes=67_000_000
        ),
        name="layer",
    )(tokens, lru_input, lru_gate, lru_output, ffn_gate, ffn_up, ffn_down, *rest)


def local(mesh_fs, *args):
    (
        tokens,
        mix_gain,
        lru_input,
        lru_gate,
        lru_input_scale,
        lru_gate_scale,
        conv_weight,
        recur_gate,
        input_gate,
        decay_rate,
        extra_decay,
        lru_output,
        lru_output_scale,
        ffn_gain,
        ffn_gate,
        ffn_up,
        ffn_gate_scale,
        ffn_up_scale,
        ffn_down,
        ffn_down_scale,
    ) = args
    ny = 2 if mesh_fs % 2 == 0 else 1
    return layer(
        ny,
        mesh_fs // ny,
        tokens,
        lru_input,
        lru_gate,
        lru_output,
        ffn_gate,
        ffn_up,
        ffn_down,
        extra_decay[None, :],
        mix_gain[None, :],
        ffn_gain[None, :],
        lru_input_scale[None, :],
        lru_gate_scale[None, :],
        lru_output_scale[None, :],
        jnp.stack([ffn_gate_scale, ffn_up_scale]),
        ffn_down_scale[None, :],
        conv_weight,
        recur_gate,
        input_gate,
        decay_rate[None, :],
    )


def solution(mesh):
    in_specs = (
        P(("rep", "fs"), "tp"),
        P(),
        P("fs", "tp"),
        P("fs", "tp"),
        P("tp"),
        P("tp"),
        P(None, "tp"),
        P("tp", None, None),
        P("tp", None, None),
        P("tp"),
        P(("rep", "fs")),
        P("tp", "fs"),
        P(),
        P(),
        P("fs", "tp"),
        P("fs", "tp"),
        P("tp"),
        P("tp"),
        P("tp", "fs"),
        P(),
    )
    out_specs = P(("rep", "fs"), "tp")
    mesh_fs = mesh.shape["fs"]
    return jax.shard_map(
        lambda *args: local(mesh_fs, *args),
        mesh=mesh,
        in_specs=in_specs,
        out_specs=out_specs,
        check_vma=False,
    )
```

time: 200 us -> 182 us (0.910)
  Pallas kernels: 196 us -> 178 us
    pallas_call x1, Pallas kernels: 196 us -> 178 us  [layer(): pl.pallas_call(functools.partial(layer_kernel, ny, nz), out_shape=jax.Sha...]
where the time goes in v1:
time: 182 us
  Pallas kernels  178 us (98%)
  local copies, waits for them, and re-layouts  3.66 us (2%)
    pallas_call x1, Pallas kernels, layer(): pl.pallas_call(functools.partial(layer_kernel, ny, nz), out_shape=jax.Sha...  178 us

profile of v1, /device:TPU:0, one launch (start us, length us, event | category | flops | bytes accessed | tf_op | source)
XLA Modules:
  0.0 181.9 jit_solution(17228968243736728646)
XLA Ops:
  0.0 0.7 stack.9
  0.7 0.7 stack.10
  1.4 0.6 pad_maximum_fusion.fscale_ref
  2.0 177.7 %layer.1 = bf16[512,1024]{1,0:T(8,128)(2,1)} custom-call(bf16[512,1024]{1,0:T(8,128)(2,1)} %tokens.1, f32[256,1024]{1,0:T(8,128)} %lru_input.1, f32[256,1024]{1,0:T(8,128)} %lru_gate.1, f32[1024,256]{1,0:T(8,128)} %lru_output.1, f32[256,1408]{1,0:T(8,128)} %ffn_gate.1, f32[256,1408]{1,0:T(8,128)} %ffn_up.1, f32[1408,256]{1,0:T(8,128)} %ffn_down.1, ...), custom_call_target="tpu_custom_call" | custom-call | tf_op jit(solution)/shard_map/layer/pallas_call | solution.py:741
  179.7 2.3 %copy.22 = bf16[512,1024]{1,0:T(8,128)(2,1)} copy(bf16[512,1024]{1,0:T(8,128)(2,1)} %layer.1) | data formatting | bytes 2097152

commit v2 on v1

--- a/solution.py
+++ b/solution.py
@@ -14,6 +14,7 @@
 RATE_BOTH = 21500.0
 EARLY = 4
 TOKENS = 39.0
+LAG = 0.0
 HOP = 22.5
 DOT = (1.5, 0.0, 2.2)
 MESH = pl.DeviceIdType.MESH
@@ -150,22 +151,22 @@
     pair = {"fs": z * ny + (1 - y)}
     give = (give_mix, give_out, give_gu, give_down)
     half = nz // 2
-    plan = ((64, 96, 96), (256, 256), (96, 96, 64))
+    plan = ((64, 96, 96), (256, 256), (96, 96, 64), (352, 352))
     groups = []
     for b, parts in enumerate(plan):
-        row, rows = 0, buf[b].shape[1]
+        row, rows = 0, buf[b].shape[-2]
         for i, n in enumerate(parts):
             n = rows - row if i + 1 == len(parts) else max(16, n * rows // sum(parts) // 16 * 16)
             groups.append((b, row, n))
             row += n
-    subs = b3.shape[1]
+    subs = part.shape[1] // hb
     cs = c // subs
-    groups += [(3, i, hidden) for i in range(subs)]
 
     clock = [0.0]
     eta, slots, at_time = {}, [], FIRST
     for g, (b, _, n) in enumerate(groups):
         size = n * buf[b].shape[-1]
+        at_time += LAG if g == EARLY + 1 else 0.0
         for k in range(1, nz):
             at_time += size / RATE_BOTH
             eta[g, k] = at_time
@@ -178,7 +179,7 @@
 
     def cut(g, ref, *at):
         b, row, rows = groups[g]
-        return ref.at[(*at, row if b == 3 else pl.ds(row, rows))]
+        return ref.at[(*at, pl.ds(row, rows))]
 
     def piece(g, at, w):
         return cut(g, buf[groups[g][0]], at * ny + (rep if w == 0 else 1 - rep))
@@ -226,14 +227,9 @@
 
     @scoped("slot")
     def slot(g, k):
-        if k == nz - 1 and g <= EARLY:
-            own_z(g + 1)
+        if k == nz - 1:
             for n in {2: (5, 6), 3: (7,), 4: (8, 9)}.get(g, ()):
                 own_y(n)
-            if g == EARLY:
-                own_z(g + 2)
-        if k == 1 and g > EARLY:
-            own_z(g + 2)
 
         @pl.when(z >= k)
         def _():
@@ -256,6 +252,9 @@
                     down_z(g, k + 1, z + k).start()
 
             over(g, nz - k).start()
+
+        if k == (max(1, nz - 2) if g <= EARLY else 1):
+            own_z(g + 1)
 
     def next_slot():
         key = slots.pop(0)
@@ -314,9 +313,6 @@
                 src = ffn_down.at[pl.ds(h * hidden + row, n), pl.ds(i * cs, cs)]
                 to = part.at[1, (h * subs + i) * len(cuts) + r, :n]
                 loads.append(stage(src, to, len(loads)))
-    for load in loads:
-        load.start()
-
     barrier = pltpu.get_barrier_semaphore()
 
     def greet(where):
@@ -328,6 +324,8 @@
     pl.when(z + 1 < nz)(lambda: greet({"fs": lax.rem(z + 1, nz) * ny + y}))
     pl.when(z > 0)(lambda: greet({"fs": lax.rem(z + nz - 1, nz) * ny + y}))
 
+    for load in loads[:3]:
+        load.start()
     loads[0].wait()
     loads[1].wait()
     for i in range(2):
@@ -349,6 +347,8 @@
     extra_x = copy(ex.at[0], ex.at[1], ts.at[3], tr.at[3], pair)
     own_y(0)
     tok_tp.start()
+    for load in loads[5:] + loads[3:5]:
+        load.start()
     extra_x.start()
     for load in loads[5 : 5 + 2 * subs]:
         load.wait()
@@ -409,11 +409,11 @@
         for load in loads[5 + 2 * subs :]:
             load.wait()
         for i in range(subs):
-            for which, to in ((y, b3.at[me, i]), (1 - y, give_down.at[i])):
+            for which, to in ((y, b3.at[me]), (1 - y, give_down)):
                 for r, row in enumerate(cuts):
                     n = min(length, hidden - row)
                     at = (which * subs + i) * len(cuts) + r
-                    to[row : row + n] = part[1, at, :n].astype(bf16)
+                    to[row : row + n, i * cs : (i + 1) * cs] = part[1, at, :n].astype(bf16)
 
     @scoped("tables")
     def tables():
@@ -485,7 +485,7 @@
 
     def from_twin(b, d, sub=0):
         for g, group in enumerate(groups):
-            if group[0] == b and (b < 3 or group[1] == sub):
+            if group[0] == b:
                 arrived(over(g, d, 1))
 
     def ready(b, i):
@@ -534,7 +534,7 @@
         theirs, mine = (1 - tp) * hb + j, tp * hb + j
 
         def product(at):
-            acts, w = (gated, b1.at[at]) if l == 0 else (hid, b3.at[at, i])
+            acts, w = (gated, b1.at[at]) if l == 0 else (hid, b3.at[at])
             return jnp.dot(acts[s], w[...], preferred_element_type=f32)
 
         def put(to, v):
@@ -634,20 +634,19 @@
     run(1.3, norm, tok_block(1), 1, mgain_ref)
     for sent in (tok_tp, tok_x, tok_xtp, extra_x):
         sent.wait_send()
-    ready(0, -1)
-    for s in (0, 1):
-        dots(0, s, -1)
-    for i in ranks[1:]:
+    clock[0] = max(clock[0], TOKENS + 6.0)
+    for i in ranks:
         ready(0, i)
-        for s in (0, 1):
-            dots(0, s, i)
+        dots(0, 1, i)
     arrived(extra_x)
     for s in (1, 0):
         for span in spans:
             run(3.3, recurrence, s, *span)
-    for i in ranks:
-        ready(1, i)
-    for s in (1, 0):
+        if s:
+            for i in ranks:
+                dots(0, 0, i)
+            for i in ranks:
+                ready(1, i)
         for j in range(hb):
             run(0.9, project, 0, s, j)
             if j:
@@ -668,35 +667,40 @@
     dots(2, 1, -1)
     for i in ranks[1:]:
         ready(2, i)
-        for s in (1, 0):
-            dots(2, s, i)
+        dots(2, 1, i)
     run(0.8, hide, 1)
-    run(0.8, hide, 0)
     for j in range(hb):
         for s in range(2):
             x_copy(0, s, j).wait_send()
     pl.semaphore_wait(free, 1)
 
-    for i in range(subs):
-        g = len(groups) - subs + i
+    def blocks_of(i):
         for w in (0, 1):
             for k in range(half):
-                d = half if k == 0 and w == 0 else nz - 1
-                while slots and slots[0] <= (g, d):
-                    next_slot()
-                if w:
-                    if k:
-                        from_twin(3, k, i)
-                    from_twin(3, k + half, i)
-                j = lax.rem(z - k + nz, half) * ny + (1 - rep if w else rep)
-                run(0.4, project, 1, 1, j, i)
-                run(0.4, project, 1, 0, j, i)
-                run(0.3, send, 1, 1, j, i)
-    for q in range(chunks):
-        finish(q)
-
-    @scoped("sent")
-    def sent_all():
+                yield w, k, lax.rem(z - k + nz, half) * ny + (1 - rep if w else rep)
+
+    def others():
+        for i in ranks[1:]:
+            dots(2, 0, i)
+        hide(0)
+
+    g = len(groups) - 1
+    for w, k, j in blocks_of(0):
+        d = half if k == 0 and w == 0 else nz - 1
+        if (w, k) == (1, 0):
+            others()
+        while slots and slots[0] <= (g, d):
+            next_slot()
+        if w:
+            if k:
+                from_twin(3, k)
+            from_twin(3, k + half)
+        project(1, 1, j)
+        send(1, 1, j)
+    for w, k, j in blocks_of(0):
+        project(1, 0, j)
+    @scoped("passed")
+    def passed():
         for g in range(len(groups)):
             for k in range(1, nz):
 
@@ -710,6 +714,13 @@
 
                 over(g, k).wait_send()
             swap(g).wait_send()
+
+    passed()
+    for q in range(chunks):
+        finish(q)
+
+    @scoped("sent")
+    def sent_all():
         for j in range(hb):
             for i in range(subs):
                 x_copy(1, 1, j, i).wait_send()
@@ -732,7 +743,7 @@
     c = lru_input.shape[0]
     hb = columns // c
     width, hidden = lru_output.shape[0] // 2, ffn_down.shape[0] // 2
-    subs = 2 if c % (2 * LANES) == 0 else 1
+    subs = 1
     cut = (hb * subs, length, c // subs)
     bf16, f32 = jnp.bfloat16, jnp.float32
     dma = pltpu.SemaphoreType.DMA
@@ -750,11 +761,11 @@
             pltpu.VMEM((fs, c, 2 * width), bf16),
             pltpu.VMEM((fs, width, c), bf16),
             pltpu.VMEM((fs, c, 2 * hidden), bf16),
-            pltpu.VMEM((fs, subs, hidden, c // subs), bf16),
+            pltpu.VMEM((fs, hidden, c), bf16),
             pltpu.VMEM((c, 2 * width), bf16),
             pltpu.VMEM((width, c), bf16),
             pltpu.VMEM((c, 2 * hidden), bf16),
-            pltpu.VMEM((subs, hidden, c // subs), bf16),
+            pltpu.VMEM((hidden, c), bf16),
             pltpu.VMEM((2, length, 2 * max(width, hidden)), f32),
             pltpu.VMEM((2, length, width), bf16),
             pltpu.VMEM((2, length, hidden), bf16),

time: 182 us -> 175 us (0.962)
  Pallas kernels: 178 us -> 171 us
    pallas_call x1, Pallas kernels: 178 us -> 171 us  [layer(): pl.pallas_call(functools.partial(layer_kernel, ny, nz), out_shape=jax.Sha...]
where the time goes in v2:
time: 175 us
  Pallas kernels  171 us (98%)
  local copies, waits for them, and re-layouts  3.66 us (2%)
    pallas_call x1, Pallas kernels, layer(): pl.pallas_call(functools.partial(layer_kernel, ny, nz), out_shape=jax.Sha...  171 us

profile of v2, /device:TPU:0, one launch (start us, length us, event | category | flops | bytes accessed | tf_op | source)
XLA Modules:
  0.0 175.2 jit_solution(1810329640058680508)
XLA Ops:
  0.0 0.7 stack.9
  0.7 0.7 stack.10
  1.4 0.6 pad_maximum_fusion.fscale_ref
  2.0 170.9 %layer.1 = bf16[512,1024]{1,0:T(8,128)(2,1)} custom-call(bf16[512,1024]{1,0:T(8,128)(2,1)} %tokens.1, f32[256,1024]{1,0:T(8,128)} %lru_input.1, f32[256,1024]{1,0:T(8,128)} %lru_gate.1, f32[1024,256]{1,0:T(8,128)} %lru_output.1, f32[256,1408]{1,0:T(8,128)} %ffn_gate.1, f32[256,1408]{1,0:T(8,128)} %ffn_up.1, f32[1408,256]{1,0:T(8,128)} %ffn_down.1, ...), custom_call_target="tpu_custom_call" | custom-call | tf_op jit(solution)/shard_map/layer/pallas_call | solution.py:752
  172.9 2.3 %copy.22 = bf16[512,1024]{1,0:T(8,128)(2,1)} copy(bf16[512,1024]{1,0:T(8,128)(2,1)} %layer.1) | data formatting | bytes 2097152
